TPU v7x, 128 devices: a whole 4x4x4 slice. The times are simulated.
128 devices in a mesh: ep: 128 (over z, y, x, core).
Axes of the slice: x: 4, y: 4, z: 4, core: 2. Of those that a mesh axis runs over, the one named last changes fastest.
Arguments:
- tokens: bfloat16 [8192, 2048], P('ep'), may hold values from -6 to 6
- conv_state: bfloat16 [8192, 3, 1024], P('ep'), may hold values from -6 to 6
- recur_state: float32 [8192, 1024], P('ep'), may hold values from -6 to 6
- w_branch: bfloat16 [2048, 1024], replicated, may hold values from -0.125 to 0.125
- w_gate: bfloat16 [2048, 1024], replicated, may hold values from -0.125 to 0.125
- conv_taps: float32 [4, 1024], replicated, may hold values from -3 to 3
- rate_blocks: bfloat16 [16, 64, 64], replicated, may hold values from -0.75 to 0.75
- input_blocks: bfloat16 [16, 64, 64], replicated, may hold values from -0.75 to 0.75
- decay_param: float32 [1024], replicated, may hold values from 1.5 to 6.5
- w_mix: bfloat16 [1024, 2048], replicated, may hold values from -0.1875 to 0.1875
- gain_pre: float32 [2048], replicated, may hold values from 0.1 to 1.9
- gain_post: float32 [2048], replicated, may hold values from 0.1 to 1.9
- gain_ffn: float32 [2048], replicated, may hold values from 0.1 to 1.9
- gain_out: float32 [2048], replicated, may hold values from 0.1 to 1.9
- routes: int32 [8192, 2], P('ep'), may hold values from 0 to 127, all different within a row; in each aligned block of 64 rows (0 to 63, 64 to 127, ...) at most 3 rows name the same one
- affinity: float32 [8192, 2], P('ep'), may hold values from 0.05 to 1
- w_expert_gate: bfloat16 [128, 2048, 512], P('ep'), may hold values from -0.125 to 0.125
- w_expert_up: bfloat16 [128, 2048, 512], P('ep'), may hold values from -0.125 to 0.125
- w_expert_down: bfloat16 [128, 512, 2048], P('ep'), may hold values from -0.25 to 0.25
Outputs:
- layer_out: bfloat16 [8192, 2048], P('ep')
- conv_next: bfloat16 [8192, 3, 1024], P('ep')
- state_next: float32 [8192, 1024], P('ep')
Inputs may be any that keep to these rules, and one draw needn't show every extreme that they name: `routes`: each row names 2 different experts. Among the 64 rows of one device no expert is named more than 3 times, and in every draw some device names some expert exactly 3 times.
All inputs are finite; a program needn't handle non-finite values.
Results may differ from a plain program's by a relative error of at most 0.014.
Values may be sent and summed in bfloat16 or wider, within the bound.
A program may use at most 128 MiB of HBM per device.

v0:
```python
import jax
import jax.numpy as jnp
from jax import lax
from jax.sharding import PartitionSpec as P

epsilon = 1e-06
gate_scale = 8.0


def norm_rows(values, gain_vec):
    floats = values.astype(jnp.float32)
    inv_scale = lax.rsqrt(jnp.mean(floats * floats, axis=-1, keepdims=True) + epsilon)
    return floats * inv_scale * gain_vec


def recurrence(
    tokens,
    conv_state,
    recur_state,
    w_branch,
    w_gate,
    conv_taps,
    rate_blocks,
    input_blocks,
    decay_param,
    w_mix,
    gain_pre,
    gain_post,
):
    normed = norm_rows(tokens, gain_pre).astype(jnp.bfloat16)
    branch = jnp.dot(normed, w_branch, preferred_element_type=jnp.float32).astype(jnp.bfloat16)
    gate_act = jnp.dot(normed, w_gate, preferred_element_type=jnp.float32).astype(jnp.bfloat16)
    window = jnp.concatenate([conv_state, branch[:, None, :]], axis=1)
    convolved = jnp.sum(window.astype(jnp.float32) * conv_taps[None], axis=1)
    row_count, branch_width = convolved.shape
    blocks = rate_blocks.shape[0]
    pieces = convolved.reshape(row_count, blocks, branch_width // blocks)
    rate_gate = jax.nn.sigmoid(
        jnp.einsum("snc,ncd->snd", pieces, rate_blocks.astype(jnp.float32)).reshape(
            row_count, branch_width
        )
    )
    inflow = jax.nn.sigmoid(
        jnp.einsum("snc,ncd->snd", pieces, input_blocks.astype(jnp.float32)).reshape(
            row_count, branch_width
        )
    )
    log_decay = -gate_scale * rate_gate * jax.nn.softplus(-decay_param)
    state_next = jnp.exp(log_decay) * recur_state + jnp.sqrt(-jnp.expm1(2.0 * log_decay)) * (
        inflow * convolved
    )
    merged = (state_next * jax.nn.gelu(gate_act.astype(jnp.float32))).astype(jnp.bfloat16)
    mix_out = jnp.dot(merged, w_mix, preferred_element_type=jnp.float32).astype(jnp.bfloat16)
    residual = tokens.astype(jnp.float32) + norm_rows(mix_out, gain_post)
    return (residual, window[:, 1:, :], state_next)


def expert_block(got_rows, got_info, cap_total, w_expert_gate, w_expert_up, w_expert_down):
    slot_count, sources, model_width = got_rows.shape
    counts = got_info[0]
    before = jnp.cumsum(counts) - counts
    allowed = jnp.clip(cap_total - before, 0, counts)
    positions = jnp.arange(slot_count, dtype=jnp.int32)
    keep_mask = positions[:, None] < allowed[None, :]
    row_block = got_rows.reshape(slot_count * sources, model_width)
    gate_part = jnp.dot(row_block, w_expert_gate[0], preferred_element_type=jnp.float32)
    up_part = jnp.dot(row_block, w_expert_up[0], preferred_element_type=jnp.float32)
    hidden = (jax.nn.silu(gate_part) * up_part).astype(jnp.bfloat16)
    outputs = jnp.dot(hidden, w_expert_down[0], preferred_element_type=jnp.float32).astype(
        jnp.bfloat16
    )
    outputs = outputs.reshape(slot_count, sources, model_width)
    return jnp.where(keep_mask[:, :, None], outputs, jnp.zeros_like(outputs))


def shards(
    tokens,
    conv_state,
    recur_state,
    w_branch,
    w_gate,
    conv_taps,
    rate_blocks,
    input_blocks,
    decay_param,
    w_mix,
    gain_pre,
    gain_post,
    gain_ffn,
    gain_out,
    routes,
    affinity,
    w_expert_gate,
    w_expert_up,
    w_expert_down,
):
    residual, conv_next, state_next = recurrence(
        tokens,
        conv_state,
        recur_state,
        w_branch,
        w_gate,
        conv_taps,
        rate_blocks,
        input_blocks,
        decay_param,
        w_mix,
        gain_pre,
        gain_post,
    )
    ffn_in = norm_rows(residual, gain_ffn).astype(jnp.bfloat16)
    seq_count, top_count = routes.shape
    model_width = ffn_in.shape[1]
    experts = lax.axis_size("ep") * w_expert_gate.shape[0]
    capacity = max(2, 3 * seq_count * top_count // lax.axis_size("ep"))
    cap_total = seq_count * top_count // 2
    flat_routes = routes.reshape(-1)
    onehot = (flat_routes[:, None] == jnp.arange(experts, dtype=jnp.int32)[None, :]).astype(
        jnp.int32
    )
    slot_index = jnp.sum(jnp.cumsum(onehot, axis=0) * onehot, axis=1) - 1
    load_counts = jnp.sum(onehot, axis=0)
    slot_target = slot_index * experts + flat_routes
    outgoing = (
        jnp.zeros((capacity * experts, model_width), jnp.bfloat16)
        .at[slot_target]
        .set(jnp.repeat(ffn_in, top_count, axis=0))
    )
    outgoing = outgoing.reshape(capacity, experts, model_width)
    send_info = load_counts[None, :]
    got_rows, got_info = (
        lax.all_to_all(outgoing, "ep", split_axis=1, concat_axis=1, tiled=True),
        lax.all_to_all(send_info, "ep", split_axis=1, concat_axis=1, tiled=True),
    )
    finished = expert_block(
        got_rows, got_info, cap_total, w_expert_gate, w_expert_up, w_expert_down
    )
    gathered = lax.all_to_all(finished, "ep", split_axis=1, concat_axis=1, tiled=True)
    picked = jnp.take(gathered.reshape(capacity * experts, model_width), slot_target, axis=0)
    picked = picked.astype(jnp.float32).reshape(seq_count, top_count, model_width)
    weights = affinity / jnp.sum(affinity, axis=1, keepdims=True)
    combined = jnp.sum(weights[:, :, None] * picked, axis=1)
    layer_out = (residual + norm_rows(combined, gain_out)).astype(jnp.bfloat16)
    return (layer_out, conv_next, state_next)


def solution(mesh):
    return jax.shard_map(
        shards,
        mesh=mesh,
        in_specs=(
            P("ep", None),
            P("ep", None, None),
            P("ep", None),
            P(),
            P(),
            P(),
            P(),
            P(),
            P(),
            P(),
            P(),
            P(),
            P(),
            P(),
            P("ep", None),
            P("ep", None),
            P("ep", None, None),
            P("ep", None, None),
            P("ep", None, None),
        ),
        out_specs=(P("ep", None), P("ep", None, None), P("ep", None)),
        check_vma=False,
    )
```

profile of v0, /device:TPU:1, one launch (start us, length us, event | category | flops | bytes accessed | tf_op | source)
XLA Modules:
  0.0 144.8 jit_solution(8652647469590497452)
XLA Ops:
  0.6 0.9 copy.69
  2.0 0.8 fusion.55
  2.7 0.7 copy.72
  3.5 11.9 %all-to-all-start = ((s32[1,128,1]{2,0,1:T(1,128)}), s32[1,128,1]{2,0,1:T(1,128)}, u32[]{:S(2)}, u32[]{:S(2)}) async-start(s32[1,128,1]{2,0,1:T(1,128)} %copy.72), calls=%async_computation | async-start | bytes 131072 | tf_op jit(solution)/shard_map/all_to_all | solution.py:133
  15.4 0.7 reshape.196
  16.1 1.1 fusion.31
  17.2 3.2 %fusion.21 = bf16[64,1,1024]{2,0,1:T(8,128)(2,1)S(1)} fusion(bf16[2048,1024]{1,0:T(8,128)(2,1)} %param.22, bf16[64,2048]{1,0:T(8,128)(2,1)} %param.19, f32[2048]{0:T(1024)} %param.29, f32[64]{0:T(128)S(1)} %add_rsqrt_fusion.3), kind=kOutput, calls=%fused_computation.26 | convolution fusion | flops 269025280 | bytes 4595968 | tf_op jit(solution)/shard_map/dot_general | solution.py:31
  21.6 1.2 fusion.19
  23.2 0.9 div.40
  24.1 1.3 multiply_add_fusion
  25.5 5.3 %multiply_reduce_fusion.4 = (f32[64]{0:T(128)S(1)}, f32[64,2048]{1,0:T(8,128)S(1)}) fusion(bf16[1024,2048]{1,0:T(8,128)(2,1)} %param.28, f32[64,1024]{1,0:T(8,128)S(1)} %multiply_add_fusion, bf16[2048,1024]{1,0:T(8,128)(2,1)} %param.23, bf16[64,2048]{1,0:T(8,128)(2,1)S(1)} %copy-done.1, f32[2048]{0:T(1024)S(1)} %copy-done.8, f32[64]{0:T(128)} %copy-done.17), kind=kOutput, calls=%fused_computation.50 | convolution fusion | flops 538705856 | bytes 9445888 | tf_op jit(solution)/shard_map/dot_general | solution.py:53
  31.7 1.0 reshape.214
  32.7 3.2 %scatter_custom_fusion = bf16[384,2048]{1,0:T(8,128)(2,1)} fusion(s32[128]{0:T(128)S(1)} %fusion.57, bf16[128,2048]{1,0:T(8,128)(2,1)} %reshape.214, bf16[]{:T(256)} %constant.60.clone.1), kind=kCustom, calls=%fused_computation.35 | custom fusion | bytes 1573376 | tf_op jit(solution)/shard_map/scatter | solution.py:127
  35.9 4.1 %copy.75 = bf16[3,128,2048]{2,0,1:T(4,128)(2,1)} copy(bf16[3,128,2048]{2,1,0:T(8,128)(2,1)} %bitcast.41) | data formatting | bytes 3145728 | tf_op jit(solution)/shard_map/reshape | solution.py:129
  40.0 10.2 %all-to-all-start.1 = ((bf16[3,128,2048]{2,0,1:T(4,128)(2,1)}), bf16[3,128,2048]{2,0,1:T(4,128)(2,1)}, u32[]{:S(2)}, u32[]{:S(2)}) async-start(bf16[3,128,2048]{2,0,1:T(4,128)(2,1)} %copy.75), calls=%async_computation.1 | async-start | bytes 4194304 | tf_op jit(solution)/shard_map/all_to_all | solution.py:132
  50.3 1.0 reduce-window.8
  51.4 3.2 %reduce = s32[128]{0:T(128)S(1)} reduce(s32[1,128,1]{2,0,1:T(1,128)} %all-to-all-done, s32[]{:T(128)} %constant.54.clone.1), dimensions={0,2}, to_apply=%all_to_all.15.reduce_sub_computation | reduce | bytes 1028 | tf_op jit(solution)/shard_map/all_to_all | solution.py:133
  54.7 25.7 %all-to-all-done.1 = bf16[3,128,2048]{2,0,1:T(4,128)(2,1)} async-done(((bf16[3,128,2048]{2,0,1:T(4,128)(2,1)}), bf16[3,128,2048]{2,0,1:T(4,128)(2,1)}, u32[]{:S(2)}, u32[]{:S(2)}) %all-to-all-start.1) | async-done | bytes 1572896 | tf_op jit(solution)/shard_map/all_to_all | solution.py:132
  80.4 2.9 %copy.76 = bf16[3,128,2048]{2,1,0:T(8,128)(2,1)S(1)} copy(bf16[3,128,2048]{2,0,1:T(4,128)(2,1)} %all-to-all-done.1) | data formatting | bytes 3145728 | tf_op jit(solution)/shard_map/all_to_all | solution.py:132
  83.3 1.1 copy-done.2
  84.4 1.9 %fusion.4 = f32[384,512]{1,0:T(8,128)} fusion(bf16[384,2048]{1,0:T(8,128)(2,1)S(1)} %bitcast.43, bf16[1,2048,512]{2,1,0:T(8,128)(2,1)S(1)} %copy-done.23), kind=kOutput, calls=%fused_computation.8 | convolution fusion | flops 805306368 | bytes 4456448 | tf_op jit(solution)/shard_map/dot_general | solution.py:66
  86.3 5.3 %convolution_convert_fusion = bf16[384,2048]{1,0:T(8,128)(2,1)} fusion(bf16[1,512,2048]{2,1,0:T(8,128)(2,1)S(1)} %copy-done, bf16[384,2048]{1,0:T(8,128)(2,1)} %bitcast.44, bf16[1,2048,512]{2,1,0:T(8,128)(2,1)} %param.36, f32[384,512]{1,0:T(8,128)} %fusion.4), kind=kOutput, calls=%fused_computation.2 | convolution fusion | flops 1612578816 | bytes 8126464 | tf_op jit(solution)/shard_map/dot_general | solution.py:69
  91.6 4.3 %copy_select_fusion = bf16[3,128,2048]{2,0,1:T(4,128)(2,1)} fusion(bf16[3,128,2048]{2,1,0:T(8,128)(2,1)} %bitcast.42, pred[3,128]{0,1:T(8,128)(4,1)S(1)} %iota_compare_fusion), kind=kLoop, calls=%fused_computation.10 | loop fusion | flops 786432 | bytes 3146112 | tf_op jit(solution)/shard_map/jit(_where)/select_n | solution.py:73
  95.9 5.6 %all-to-all-start.2 = ((bf16[3,128,2048]{2,0,1:T(4,128)(2,1)}), bf16[3,128,2048]{2,0,1:T(4,128)(2,1)}, u32[]{:S(2)}, u32[]{:S(2)}) async-start(bf16[3,128,2048]{2,0,1:T(4,128)(2,1)} %copy_select_fusion), calls=%async_computation.2 | async-start | bytes 4194304 | tf_op jit(solution)/shard_map/all_to_all | solution.py:138
  102.0 0.7 copy.68
  103.3 0.8 fusion.36
  104.1 27.7 %all-to-all-done.2 = bf16[3,128,2048]{2,0,1:T(4,128)(2,1)} async-done(((bf16[3,128,2048]{2,0,1:T(4,128)(2,1)}), bf16[3,128,2048]{2,0,1:T(4,128)(2,1)}, u32[]{:S(2)}, u32[]{:S(2)}) %all-to-all-start.2) | async-done | bytes 1572896 | tf_op jit(solution)/shard_map/all_to_all | solution.py:138
  131.8 3.9 %copy.78 = bf16[3,128,2048]{2,1,0:T(8,128)(2,1)} copy(bf16[3,128,2048]{2,0,1:T(4,128)(2,1)} %all-to-all-done.2) | data formatting | bytes 3145728 | tf_op jit(solution)/shard_map/all_to_all | solution.py:138
  135.7 3.2 %gather_fusion = bf16[128,2048]{1,0:T(8,128)(2,1)S(1)} fusion(bf16[384,2048]{1,0:T(8,128)(2,1)} %bitcast.40, s32[1024]{0:T(1024)} %pad_clamp_fusion), kind=kCustom, calls=%fused_computation | custom fusion | bytes 1049088 | tf_op jit(solution)/shard_map/jit(_take)/gather | solution.py:139
  138.9 1.1 gather.7
  140.0 3.7 %multiply_reduce_fusion = f32[64,2048]{1,0:T(8,128)S(1)} fusion(bf16[64,2,2048]{2,1,0:T(2,128)(2,1)} %gather.7, pred[64,2]{1,0:T(8,128)(4,1)S(1)} %copy.71, f32[64,2]{1,0:T(8,128)S(1)} %copy-done.6), kind=kLoop, calls=%fused_computation.27 | loop fusion | flops 917504 | bytes 1049216 | tf_op jit(solution)/shard_map/reduce_sum | solution.py:142
  143.9 0.9 add_convert_fusion
  (80 shorter events, 4.1 us)
Async XLA Ops:
  0.6 85.6 %copy-start = (bf16[1,512,2048]{2,1,0:T(8,128)(2,1)S(1)}, bf16[1,512,2048]{2,1,0:T(8,128)(2,1)}, u32[]{:S(2)}) copy-start(bf16[1,512,2048]{2,1,0:T(8,128)(2,1)} %param.37) | copy-start | bytes 6291460
  3.5 36.6 %all-to-all-start = ((s32[1,128,1]{2,0,1:T(1,128)}), s32[1,128,1]{2,0,1:T(1,128)}, u32[]{:S(2)}, u32[]{:S(2)}) async-start(s32[1,128,1]{2,0,1:T(1,128)} %copy.72), calls=%async_computation | async-start | bytes 131072 | tf_op jit(solution)/shard_map/all_to_all | solution.py:133
  17.2 3.3 %copy-start.17 = (f32[64]{0:T(128)}, f32[64]{0:T(128)S(1)}, u32[]{:S(2)}) copy-start(f32[64]{0:T(128)S(1)} %add_rsqrt_fusion.3) | copy-start | bytes 772
  17.2 3.3 %copy-start.3 = (bf16[64,3,1024]{2,0,1:T(8,128)(2,1)S(1)}, bf16[64,3,1024]{2,0,1:T(8,128)(2,1)}, u32[]{:S(2)}) copy-start(bf16[64,3,1024]{2,0,1:T(8,128)(2,1)} %param.20) | copy-start | bytes 1179652
  17.2 3.3 %copy-start.9 = (f32[4,1024]{1,0:T(4,128)S(1)}, f32[4,1024]{1,0:T(4,128)}, u32[]{:S(2)}) copy-start(f32[4,1024]{1,0:T(4,128)} %param.24) | copy-start | bytes 49156
  17.2 3.6 %copy-start.24 = (bf16[16,64,64]{2,1,0:T(8,128)(2,1)S(1)}, bf16[16,64,64]{2,1,0:T(8,128)(2,1)}, u32[]{:S(2)}) copy-start(bf16[16,64,64]{2,1,0:T(8,128)(2,1)} %param.25) | copy-start | bytes 393220
  21.6 2.5 %copy-start.15 = (f32[1024]{0:T(1024)S(1)}, f32[1024]{0:T(1024)}, u32[]{:S(2)}) copy-start(f32[1024]{0:T(1024)} %param.27) | copy-start | bytes 12292
  22.9 2.5 %copy-start.1 = (bf16[64,2048]{1,0:T(8,128)(2,1)S(1)}, bf16[64,2048]{1,0:T(8,128)(2,1)}, u32[]{:S(2)}) copy-start(bf16[64,2048]{1,0:T(8,128)(2,1)} %param.19) | copy-start | bytes 786436
  22.9 2.5 %copy-start.8 = (f32[2048]{0:T(1024)S(1)}, f32[2048]{0:T(1024)}, u32[]{:S(2)}) copy-start(f32[2048]{0:T(1024)} %param.29) | copy-start | bytes 24580
  25.4 5.4 %copy-start.5 = (f32[64,1024]{1,0:T(8,128)}, f32[64,1024]{1,0:T(8,128)S(1)}, u32[]{:S(2)}) copy-start(f32[64,1024]{1,0:T(8,128)S(1)} %multiply_add_fusion) | copy-start | bytes 786436
  25.4 5.4 %copy-start.7 = (f32[2048]{0:T(1024)S(1)}, f32[2048]{0:T(1024)}, u32[]{:S(2)}) copy-start(f32[2048]{0:T(1024)} %param.30) | copy-start | bytes 24580
  25.4 5.7 %copy-start.10 = (f32[2048]{0:T(1024)S(1)}, f32[2048]{0:T(1024)}, u32[]{:S(2)}) copy-start(f32[2048]{0:T(1024)} %param.31) | copy-start | bytes 24580
  25.4 5.9 %copy-start.18 = (s32[128]{0:T(128)S(1)}, s32[128]{0:T(128)}, u32[]{:S(2)}) copy-start(s32[128]{0:T(128)} %get-tuple-element.4) | copy-start | bytes 1540
  25.4 5.9 %copy-start.20 = (s32[128,1]{0,1:T(1,128)S(1)}, s32[128,1]{0,1:T(1,128)}, u32[]{:S(2)}) copy-start(s32[128,1]{0,1:T(1,128)} %reshape.196) | copy-start | bytes 1540
  30.8 0.5 copy-start.12
  31.4 8.7 %copy-start.21 = (s32[128]{0:T(128)}, s32[128]{0:T(128)S(1)}, u32[]{:S(2)}) copy-start(s32[128]{0:T(128)S(1)} %fusion.57) | copy-start | bytes 1540
  40.0 40.3 %all-to-all-start.1 = ((bf16[3,128,2048]{2,0,1:T(4,128)(2,1)}), bf16[3,128,2048]{2,0,1:T(4,128)(2,1)}, u32[]{:S(2)}, u32[]{:S(2)}) async-start(bf16[3,128,2048]{2,0,1:T(4,128)(2,1)} %copy.75), calls=%async_computation.1 | async-start | bytes 4194304 | tf_op jit(solution)/shard_map/all_to_all | solution.py:132
  80.4 4.0 %copy-start.23 = (bf16[1,2048,512]{2,1,0:T(8,128)(2,1)S(1)}, bf16[1,2048,512]{2,1,0:T(8,128)(2,1)}, u32[]{:S(2)}) copy-start(bf16[1,2048,512]{2,1,0:T(8,128)(2,1)} %param.35) | copy-start | bytes 6291460
  83.3 1.1 copy-start.2
  95.9 5.7 %copy-start.19 = (s32[128]{0:T(128)S(1)}, s32[128]{0:T(128)}, u32[]{:S(2)}) copy-start(s32[128]{0:T(128)} %get-tuple-element.4) | copy-start | bytes 1540
  95.9 5.9 %copy-start.14 = (s32[64,2]{0,1:T(2,128)S(1)}, s32[64,2]{0,1:T(2,128)}, u32[]{:S(2)}) copy-start(s32[64,2]{0,1:T(2,128)} %param.33) | copy-start | bytes 1540
  95.9 6.0 %copy-start.16 = (f32[64,2]{0,1:T(2,128)S(1)}, f32[64,2]{0,1:T(2,128)}, u32[]{:S(2)}) copy-start(f32[64,2]{0,1:T(2,128)} %param.34) | copy-start | bytes 1540
  95.9 6.8 %copy-start.22 = (s32[128]{0:T(128)S(1)}, s32[128]{0:T(128)}, u32[]{:S(2)}) copy-start(s32[128]{0:T(128)} %copy-done.21) | copy-start | bytes 1540
  95.9 7.4 %copy-start.4 = (bf16[64,3,1024]{2,0,1:T(8,128)(2,1)S(1)}, bf16[64,3,1024]{2,0,1:T(8,128)(2,1)}, u32[]{:S(2)}) copy-start(bf16[64,3,1024]{2,0,1:T(8,128)(2,1)} %param.20) | copy-start | bytes 1179652
  95.9 35.9 %all-to-all-start.2 = ((bf16[3,128,2048]{2,0,1:T(4,128)(2,1)}), bf16[3,128,2048]{2,0,1:T(4,128)(2,1)}, u32[]{:S(2)}, u32[]{:S(2)}) async-start(bf16[3,128,2048]{2,0,1:T(4,128)(2,1)} %copy_select_fusion), calls=%async_computation.2 | async-start | bytes 4194304 | tf_op jit(solution)/shard_map/all_to_all | solution.py:138
  135.7 4.3 %copy-start.6 = (f32[64,2]{1,0:T(8,128)S(1)}, f32[64,2]{1,0:T(8,128)}, u32[]{:S(2)}) copy-start(f32[64,2]{1,0:T(8,128)} %copy.68) | copy-start | bytes 1540
  138.9 5.0 %copy-start.11 = (f32[2048]{0:T(1024)S(1)}, f32[2048]{0:T(1024)}, u32[]{:S(2)}) copy-start(f32[2048]{0:T(1024)} %param.32) | copy-start | bytes 24580
  138.9 5.0 %copy-start.13 = (f32[64]{0:T(128)S(1)}, f32[64]{0:T(128)}, u32[]{:S(2)}) copy-start(f32[64]{0:T(128)} %copy-done.12) | copy-start | bytes 772
where the time goes:
time: 145 us
  waiting for transfers between devices  53.4 us (37%)
  starting transfers between devices  27.8 us (19%)
  local copies, waits for them, and re-layouts  26.3 us (18%)
  other arithmetic  18.9 us (13%)
  matrix products  17.2 us (12%)
    all_to_all x1, waiting for transfers between devices, shards(): lax.all_to_all(finished, 'ep', split_axis=1, concat_axis=1, tiled=True)  27.7 us
    all_to_all x1, waiting for transfers between devices, shards(): lax.all_to_all(outgoing, 'ep', split_axis=1, concat_axis=1, tiled=True)  25.7 us
    all_to_all x1, starting transfers between devices, shards(): lax.all_to_all(send_info, 'ep', split_axis=1, concat_axis=1, tiled=True)  11.9 us
    all_to_all x1, starting transfers between devices, shards(): lax.all_to_all(outgoing, 'ep', split_axis=1, concat_axis=1, tiled=True)  10.2 us
    all_to_all x1, starting transfers between devices, shards(): lax.all_to_all(finished, 'ep', split_axis=1, concat_axis=1, tiled=True)  5.63 us
    dot_general x1, matrix products, recurrence(): jnp.dot(merged, w_mix, preferred_element_type=jnp.float32)  5.33 us
    dot_general x1, matrix products, expert_block(): jnp.dot(hidden, w_expert_down[0], preferred_element_type=jnp.float32)  5.3 us
    select_n x1, other arithmetic, expert_block(): return jnp.where(keep_mask[:, :, None], outputs, jnp.zeros_like(outputs))  4.32 us
  transfers between devices with their start and end apart: 3, of which 2 were waited for; matrix products, arithmetic and copies ran while one was open for 21% of the time, Pallas kernels for 0%

commit v1 on v0

v1 whole, which is shorter than its diff:
```python
import functools

import jax
import jax.numpy as jnp
from jax import lax
from jax.experimental import pallas as pl
from jax.experimental.pallas import tpu as pltpu
from jax.sharding import PartitionSpec as P

MESH = pl.DeviceIdType.MESH
EPS = 1e-06
DECAY = 8.0
LIMIT = 64
SLOTS = 3
F32 = jnp.float32
BF16 = jnp.bfloat16
I32 = jnp.int32


def dot(a, b):
    return jnp.dot(a, b, preferred_element_type=F32)


def inv_rms(values):
    return lax.rsqrt(jnp.mean(values * values, axis=-1, keepdims=True) + EPS)


def minus_expm1(y):
    series = y * (1.0 + y * (1 / 2 + y * (1 / 6 + y * (1 / 24 + y * (1 / 120)))))
    return -jnp.where(y > -0.1, series, jnp.exp(y) - 1.0)


def layer_kernel(
    n,
    tokens,
    conv_in,
    recur,
    taps,
    decay,
    rate_b,
    input_b,
    g_pre,
    g_post,
    g_ffn,
    g_out,
    routes,
    affinity,
    wb_hbm,
    wg_hbm,
    wm_hbm,
    eg_hbm,
    eu_hbm,
    ed_hbm,
    out,
    conv_out,
    state_out,
    wb,
    wg,
    wm,
    eg,
    eu,
    ed,
    bd,
    residual,
    tiles32,
    tiles,
    send,
    recv,
    back,
    xb,
    counts,
    all_counts,
    table_v,
    table_s,
    meta_v,
    meta_s,
    weight_v,
    weight_s,
    w_sem,
    t_sem,
    cs_sem,
    cr_sem,
    ps_sem,
    pr_sem,
    bs_sem,
    br_sem,
):
    me = lax.axis_index("ep")
    rows, width = tokens.shape
    chunks = width // 128

    loads = [
        pltpu.make_async_copy(src, dst, w_sem.at[i])
        for i, (src, dst) in enumerate(
            ((wb_hbm, wb), (wg_hbm, wg), (wm_hbm, wm), (eg_hbm, eg), (eu_hbm, eu), (ed_hbm, ed))
        )
    ]
    for load in loads:
        load.start()

    barrier = pltpu.get_barrier_semaphore()

    def greet(i, carry):
        peer = lax.rem(me + i, n)
        pl.semaphore_signal(barrier, inc=1, device_id=(peer,), device_id_type=MESH)
        return carry

    lax.fori_loop(1, n, greet, 0)

    r0, r1 = routes[0:1, :], routes[1:2, :]
    sub = lax.broadcasted_iota(I32, (rows, rows), 0)
    lane = lax.broadcasted_iota(I32, (rows, rows), 1)
    diag = sub == lane

    def column(row):
        return jnp.sum(jnp.where(diag, row, jnp.zeros_like(row)), axis=1, keepdims=True)

    def as_row(col):
        return jnp.sum(jnp.where(diag, col, jnp.zeros_like(col)), axis=0, keepdims=True)

    experts = lax.broadcasted_iota(I32, (rows, n), 1)
    token_of = lax.broadcasted_iota(I32, (rows, n), 0)
    m0, m1 = column(r0) == experts, column(r1) == experts
    both = m0 | m1
    before = dot((lane < sub).astype(F32), both.astype(F32)).astype(I32)
    counts[...] = jnp.sum(both.astype(I32), axis=0, keepdims=True)
    table_v[...] = jnp.zeros_like(table_v)
    for s in range(SLOTS):
        table_v[s : s + 1, :] = jnp.sum(
            jnp.where(both & (before == s), token_of, 0), axis=0, keepdims=True
        )
    for j, m in enumerate((m0, m1)):
        where_at = jnp.sum(jnp.where(m, experts * SLOTS + before, 0), axis=1, keepdims=True)
        table_v[SLOTS + j : SLOTS + j + 1, 0:rows] = as_row(where_at)
    table_copy = pltpu.make_async_copy(table_v, table_s, t_sem)
    table_copy.start()

    spread = (
        lax.broadcasted_iota(I32, (64, 256), 1) % 64 == lax.broadcasted_iota(I32, (64, 256), 0)
    ).astype(BF16)
    keep = (lax.broadcasted_iota(I32, (256, 256), 0) // 64) == (
        lax.broadcasted_iota(I32, (256, 256), 1) // 64
    )
    for k, blocks in enumerate((rate_b, input_b)):
        for g in range(4):
            wide = dot(blocks[256 * g : 256 * (g + 1), :], spread)
            bd[k, g] = jnp.where(keep, wide, 0.0).astype(BF16)

    tok = tokens[...].astype(F32)
    normed = (tok * inv_rms(tok) * g_pre[...]).astype(BF16)
    loads[0].wait()
    branch = dot(normed, wb[...]).astype(BF16)
    conv = branch.astype(F32) * taps[3:4, :]
    for k in range(3):
        conv = conv + conv_in[k].astype(F32) * taps[k : k + 1, :]
    conv_out[0] = conv_in[1]
    conv_out[1] = conv_in[2]
    conv_out[2] = branch
    conv_b = conv.astype(BF16)
    loads[1].wait()
    gate = dot(normed, wg[...]).astype(BF16).astype(F32)
    d = decay[...]
    soft = jnp.maximum(-d, 0.0) + jnp.log1p(jnp.exp(-jnp.abs(d)))
    merged = []
    for g in range(4):
        cols = slice(256 * g, 256 * (g + 1))
        rate = jax.nn.sigmoid(dot(conv_b[:, cols], bd[0, g]))
        inflow = jax.nn.sigmoid(dot(conv_b[:, cols], bd[1, g]))
        log_decay = -DECAY * rate * soft[:, cols]
        state = jnp.exp(log_decay) * recur[:, cols] + jnp.sqrt(minus_expm1(2.0 * log_decay)) * (
            inflow * conv[:, cols]
        )
        state_out[:, cols] = state
        x = gate[:, cols]
        gelu = 0.5 * x * (1.0 + jnp.tanh(0.7978845608028654 * (x + 0.044715 * (x * x * x))))
        merged.append((state * gelu).astype(BF16))
    merged = jnp.concatenate(merged, axis=1)
    loads[2].wait()
    mix = dot(merged, wm[...]).astype(BF16).astype(F32)
    res = tok + mix * inv_rms(mix) * g_post[...]
    residual[...] = res
    ffn = res * inv_rms(res) * g_ffn[...]

    pl.semaphore_wait(barrier, n - 1)

    def send_counts(i, carry):
        peer = lax.rem(me + i, n)
        pltpu.make_async_remote_copy(
            src_ref=counts,
            dst_ref=all_counts.at[pl.ds(me, 1)],
            send_sem=cs_sem,
            recv_sem=cr_sem,
            device_id=(peer,),
            device_id_type=MESH,
        ).start()
        return carry

    lax.fori_loop(1, n, send_counts, 0)
    all_counts[pl.ds(me, 1), :] = counts[...]

    for c in range(chunks):
        tiles32[pl.ds(c, rows, stride=chunks), :] = ffn[:, 128 * c : 128 * (c + 1)]

    def to_tiles(t, carry):
        at = pl.multiple_of(t * chunks, chunks)
        tiles[t] = tiles32[pl.ds(at, chunks), :].astype(BF16)
        return carry

    lax.fori_loop(0, rows, to_tiles, 0, unroll=8)
    table_copy.wait()

    def pick(e, carry):
        for s in range(SLOTS):
            send[e, s] = tiles[jnp.clip(table_s[s, e], 0, rows - 1)]
        return carry

    lax.fori_loop(0, n, pick, 0, unroll=8)

    def exchange(source, target, ssem, rsem):
        def start(i, carry):
            peer = lax.rem(me + lax.rem(i * 5, n), n)
            pltpu.make_async_remote_copy(
                src_ref=source.at[peer],
                dst_ref=target.at[me],
                send_sem=ssem,
                recv_sem=rsem,
                device_id=(peer,),
                device_id_type=MESH,
            ).start()
            return carry

        lax.fori_loop(1, n, start, 0)
        target[me] = source[me]

    def total(buffer, ssem, rsem):
        part = buffer.at[pl.ds(0, n - 1)]
        return pltpu.make_async_remote_copy(
            src_ref=part,
            dst_ref=part,
            send_sem=ssem,
            recv_sem=rsem,
            device_id=(lax.rem(me + 1, n),),
            device_id_type=MESH,
        )

    exchange(send, recv, ps_sem, pr_sem)

    count_sum = total(all_counts, cs_sem, cr_sem)
    count_sum.wait_recv()
    every = all_counts[...]
    sub_n = lax.broadcasted_iota(I32, (n, n), 0)
    lane_n = lax.broadcasted_iota(I32, (n, n), 1)
    own_col = jnp.sum(jnp.where(lane_n == me, every, 0), axis=1, keepdims=True)
    own_row = jnp.sum(jnp.where(lane_n == sub_n, own_col, 0), axis=0, keepdims=True)
    first_col = jnp.sum(jnp.where(lane_n < sub_n, own_row, 0), axis=1, keepdims=True)
    first_row = jnp.sum(jnp.where(sub_n < lane_n, own_col, 0), axis=0, keepdims=True)
    hit = (first_col <= lane_n) & (lane_n < first_col + own_col)
    meta_v[...] = jnp.zeros_like(meta_v)
    meta_v[0:1, :] = jnp.sum(
        jnp.where(hit, SLOTS * sub_n + lane_n - first_col, 0), axis=0, keepdims=True
    )
    for s in range(SLOTS):
        meta_v[1 + s : 2 + s, :] = jnp.minimum(first_row + s, LIMIT - 1)
    meta_copy = pltpu.make_async_copy(meta_v, meta_s, t_sem)
    meta_copy.start()

    base = jnp.sum(jnp.where(sub_n < me, every, 0), axis=0, keepdims=True)
    fits = (base + before) < LIMIT
    a0, a1 = affinity[0:1, :], affinity[1:2, :]
    weight_v[...] = jnp.zeros_like(weight_v)
    for j, (m, a) in enumerate(((m0, a0), (m1, a1))):
        kept = jnp.sum(jnp.where(m & fits, 1.0, 0.0), axis=1, keepdims=True)
        weight_v[j : j + 1, 0:rows] = as_row(kept) * (a / (a0 + a1))
    meta_copy.wait()
    weight_copy = pltpu.make_async_copy(weight_v, weight_s, t_sem)
    weight_copy.start()

    for load in loads[3:]:
        load.wait()
    rows_sum = total(recv, ps_sem, pr_sem)
    rows_sum.wait_recv()

    recv_rows = recv.reshape(n * SLOTS, chunks, 128)

    def accept(r, carry):
        at = pl.multiple_of(r * chunks, chunks)
        tiles32[pl.ds(at, chunks), :] = recv_rows[jnp.clip(meta_s[0, r], 0, n * SLOTS - 1)].astype(F32)
        return carry

    lax.fori_loop(0, LIMIT, accept, 0, unroll=8)
    for c in range(chunks):
        xb[:, 128 * c : 128 * (c + 1)] = tiles32[pl.ds(c, LIMIT, stride=chunks), :].astype(BF16)
    x = xb[...]
    hidden = (jax.nn.silu(dot(x, eg[...])) * dot(x, eu[...])).astype(BF16)
    result = dot(hidden, ed[...])
    for c in range(chunks):
        tiles32[pl.ds(c, LIMIT, stride=chunks), :] = result[:, 128 * c : 128 * (c + 1)]
    lax.fori_loop(0, LIMIT, to_tiles, 0, unroll=8)

    rows_sum.wait_send()

    def give(e, carry):
        for s in range(SLOTS):
            send[e, s] = tiles[jnp.clip(meta_s[1 + s, e], 0, LIMIT - 1)]
        return carry

    lax.fori_loop(0, n, give, 0, unroll=8)
    exchange(send, back, bs_sem, br_sem)
    weight_copy.wait()
    back_sum = total(back, bs_sem, br_sem)
    back_sum.wait_recv()

    back_rows = back.reshape(n * SLOTS, chunks, 128)

    def combine(t, carry):
        first = back_rows[jnp.clip(table_s[SLOTS, t], 0, n * SLOTS - 1)].astype(F32) * weight_s[0, t]
        second = back_rows[jnp.clip(table_s[SLOTS + 1, t], 0, n * SLOTS - 1)].astype(F32) * weight_s[1, t]
        at = pl.multiple_of(t * chunks, chunks)
        tiles32[pl.ds(at, chunks), :] = first + second
        return carry

    lax.fori_loop(0, rows, combine, 0, unroll=8)
    parts = [tiles32[pl.ds(c, rows, stride=chunks), :] for c in range(chunks)]
    combined = jnp.concatenate(parts, axis=1)
    out[...] = (residual[...] + combined * inv_rms(combined) * g_out[...]).astype(BF16)
    back_sum.wait_send()
    count_sum.wait_send()


def shards(
    n,
    tokens,
    conv_state,
    recur_state,
    w_branch,
    w_gate,
    conv_taps,
    rate_blocks,
    input_blocks,
    decay_param,
    w_mix,
    gain_pre,
    gain_post,
    gain_ffn,
    gain_out,
    routes,
    affinity,
    w_expert_gate,
    w_expert_up,
    w_expert_down,
):
    rows, width = tokens.shape
    bw = recur_state.shape[1]
    ff = w_expert_gate.shape[2]
    chunks = width // 128
    vmem = pl.BlockSpec(memory_space=pltpu.VMEM)
    hbm = pl.BlockSpec(memory_space=pl.ANY)
    dma = pltpu.SemaphoreType.DMA
    layer_out, conv_next, state_next = pl.pallas_call(
        functools.partial(layer_kernel, n),
        out_shape=(
            jax.ShapeDtypeStruct((rows, width), BF16),
            jax.ShapeDtypeStruct((3, rows, bw), BF16),
            jax.ShapeDtypeStruct((rows, bw), F32),
        ),
        in_specs=[vmem] * 13 + [hbm] * 6,
        out_specs=(vmem, vmem, vmem),
        scratch_shapes=[
            pltpu.VMEM((width, bw), BF16),
            pltpu.VMEM((width, bw), BF16),
            pltpu.VMEM((bw, width), BF16),
            pltpu.VMEM((width, ff), BF16),
            pltpu.VMEM((width, ff), BF16),
            pltpu.VMEM((ff, width), BF16),
            pltpu.VMEM((2, 4, 256, 256), BF16),
            pltpu.VMEM((rows, width), F32),
            pltpu.VMEM((rows * chunks + chunks, 128), F32),
            pltpu.VMEM((rows, chunks, 128), BF16),
            pltpu.VMEM((n, SLOTS, chunks, 128), BF16),
            pltpu.VMEM((n, SLOTS, chunks, 128), BF16),
            pltpu.VMEM((n, SLOTS, chunks, 128), BF16),
            pltpu.VMEM((LIMIT, width), BF16),
            pltpu.VMEM((1, n), I32),
            pltpu.VMEM((n, n), I32),
            pltpu.VMEM((8, 128), I32),
            pltpu.SMEM((8, 128), I32),
            pltpu.VMEM((8, 128), I32),
            pltpu.SMEM((8, 128), I32),
            pltpu.VMEM((8, 128), F32),
            pltpu.SMEM((8, 128), F32),
            dma((6,)),
            dma,
            dma,
            dma,
            dma,
            dma,
            dma,
            dma,
        ],
        compiler_params=pltpu.CompilerParams(
            collective_id=0, has_side_effects=True, vmem_limit_bytes=60 * 1024 * 1024
        ),
        name="layer",
    )(
        tokens,
        conv_state.transpose(1, 0, 2),
        recur_state,
        conv_taps,
        decay_param.reshape(1, bw),
        rate_blocks.reshape(bw, -1),
        input_blocks.reshape(bw, -1),
        gain_pre.reshape(1, width),
        gain_post.reshape(1, width),
        gain_ffn.reshape(1, width),
        gain_out.reshape(1, width),
        routes.T,
        affinity.T,
        w_branch,
        w_gate,
        w_mix,
        w_expert_gate.reshape(width, ff),
        w_expert_up.reshape(width, ff),
        w_expert_down.reshape(ff, width),
    )
    return (layer_out, conv_next.transpose(1, 0, 2), state_next)


def solution(mesh):
    row, cube, whole = P("ep", None), P("ep", None, None), P()
    return jax.shard_map(
        functools.partial(shards, mesh.shape["ep"]),
        mesh=mesh,
        in_specs=(row, cube, row) + (whole,) * 11 + (row, row, cube, cube, cube),
        out_specs=(row, cube, row),
        check_vma=False,
    )
```

time: 145 us -> 66.1 us (0.46)
  Pallas kernels: 0 us -> 60.1 us
  waiting for transfers between devices: 53.4 us -> 0 us
  starting transfers between devices: 27.8 us -> 0 us
  local copies, waits for them, and re-layouts: 26.3 us -> 5.11 us
  other arithmetic: 18.9 us -> 0 us
  matrix products: 17.2 us -> 0 us
    pallas_call x0 -> x1, Pallas kernels: none -> 60.1 us  [shards(): pl.pallas_call(functools.partial(layer_kernel, n), out_shape=(jax.ShapeDt...]
    all_to_all x3 -> x0, waiting for transfers between devices: 53.4 us -> none  [the longest x1 27.7 us: shards(): lax.all_to_all(finished, 'ep', split_axis=1, concat_axis=1, tiled=True)]
    all_to_all x3 -> x0, starting transfers between devices: 27.8 us -> none  [the longest x1 11.9 us: shards(): lax.all_to_all(send_info, 'ep', split_axis=1, concat_axis=1, tiled=True)]
    dot_general x6 -> x0, matrix products: 17.2 us -> none  [the longest x1 5.33 us: recurrence(): jnp.dot(merged, w_mix, preferred_element_type=jnp.float32)]
    all_to_all x3 -> x0, local copies, waits for them, and re-layouts: 7.5 us -> none  [the longest x1 3.88 us: shards(): lax.all_to_all(finished, 'ep', split_axis=1, concat_axis=1, tiled=True)]
    reduce_sum x7 -> x0, other arithmetic: 6.07 us -> none  [the longest x1 3.67 us: shards(): combined = jnp.sum(weights[:, :, None] * picked, axis=1)]
    reshape x4 -> x0, local copies, waits for them, and re-layouts: 5.95 us -> none  [the longest x1 4.11 us: shards(): outgoing = outgoing.reshape(capacity, experts, model_width)]
    select_n x2 -> x0, other arithmetic: 4.32 us -> none  [the longest x1 4.32 us: expert_block(): return jnp.where(keep_mask[:, :, None], outputs, jnp.zeros_like(outputs))]
  transfers between devices with their start and end apart: 3 -> 0, of which waited for: 2 -> 0; matrix products, arithmetic and copies ran while one was open for 21% -> 0% of each run, Pallas kernels for 0% -> 0%
where the time goes in v1:
time: 66.1 us; the launch traced here: 65.8 us
  Pallas kernels  60.1 us (91%)
  local copies, waits for them, and re-layouts  5.11 us (8%)
    pallas_call x1, Pallas kernels, shards(): pl.pallas_call(functools.partial(layer_kernel, n), out_shape=(jax.ShapeDt...  60.1 us
    unnamed x3, local copies, waits for them, and re-layouts  5.11 us

profile of v1, /device:TPU:1, one launch (start us, length us, event | category | flops | bytes accessed | tf_op | source)
XLA Modules:
  0.0 65.8 jit_solution(820401977812329871)
XLA Ops:
  0.6 60.1 %layer.1 = (bf16[64,2048]{1,0:T(8,128)(2,1)}, bf16[3,64,1024]{2,1,0:T(8,128)(2,1)}, f32[64,1024]{1,0:T(8,128)}) custom-call(bf16[64,2048]{1,0:T(8,128)(2,1)} %tokens.1, bf16[3,64,1024]{2,1,0:T(8,128)(2,1)} %bitcast.18, f32[64,1024]{1,0:T(8,128)} %recur.1, f32[4,1024]{1,0:T(4,128)} %taps.1, f32[1,1024]{1,0:T(1,128)} %bitcast.25, bf16[1024,64]{1,0:T(8,128)(2,1)} %bitcast.19, ...), custom_call_target="tpu_custom_call" | custom-call | tf_op jit(solution)/shard_map/layer/pallas_call | solution.py:359
  60.7 1.7 %copy.25 = bf16[64,2048]{1,0:T(8,128)(2,1)} copy(bf16[64,2048]{1,0:T(8,128)(2,1)} %get-tuple-element.12) | data formatting | bytes 524288
  62.4 1.8 %copy.26 = bf16[64,3,1024]{2,0,1:T(8,128)(2,1)} copy(bf16[64,3,1024]{2,0,1:T(8,128)(2,1)} %bitcast.17) | data formatting | bytes 786432
  64.1 1.7 %copy.27 = f32[64,1024]{1,0:T(8,128)} copy(f32[64,1024]{1,0:T(8,128)} %get-tuple-element.14) | data formatting | bytes 524288

commit v2 on v1

v2 whole, which is shorter than its diff:
```python
import functools

import jax
import jax.numpy as jnp
from jax import lax
from jax.experimental import pallas as pl
from jax.experimental.pallas import tpu as pltpu
from jax.sharding import PartitionSpec as P

MESH = pl.DeviceIdType.MESH
EPS = 1e-06
DECAY = 8.0
LIMIT = 64
SLOTS = 3
F32 = jnp.float32
BF16 = jnp.bfloat16
I32 = jnp.int32


def dot(a, b):
    return jnp.dot(a, b, preferred_element_type=F32)


def inv_rms(values):
    return lax.rsqrt(jnp.mean(values * values, axis=-1, keepdims=True) + EPS)


def minus_expm1(y):
    series = y * (1.0 + y * (1 / 2 + y * (1 / 6 + y * (1 / 24 + y * (1 / 120)))))
    return -jnp.where(y > -0.1, series, jnp.exp(y) - 1.0)


SCOPES = []


def scope(name):
    if SCOPES:
        SCOPES.pop().__exit__(None, None, None)
    if name:
        SCOPES.append(jax.named_scope(name))
        SCOPES[-1].__enter__()


def moved(device, step, sign):
    z, y, x, core = step
    return (
        (((device >> 5) + sign * z) & 3) << 5
        | (((device >> 3) + sign * y) & 3) << 3
        | (((device >> 1) + sign * x) & 3) << 1
        | ((device & 1) ^ core)
    )


def step_of(half, q):
    return ((q >> 5) * 2 + (1 - half), (q >> 3) & 3, (q >> 1) & 3, q & 1)


HALF = 64
GROUP = 8
TURN = 37


def layer_kernel(
    n,
    tokens_h,
    conv_h,
    recur_h,
    taps_h,
    decay_h,
    rate_h,
    input_h,
    g_pre_h,
    g_post_h,
    g_ffn_h,
    g_out_h,
    routes_h,
    affinity_h,
    wb_h,
    wg_h,
    wm_h,
    eg_h,
    eu_h,
    ed_h,
    out,
    conv_out,
    state_out,
    tokens,
    conv_in,
    recur,
    taps,
    decay,
    rate_b,
    input_b,
    g_pre,
    g_post,
    g_ffn,
    g_out,
    routes,
    affinity,
    wb,
    wg,
    wm,
    eg,
    eu,
    ed,
    branch_v,
    state_v,
    bd,
    residual,
    tiles32,
    tiles,
    send,
    recv_a,
    recv_b,
    ret_a,
    ret_b,
    back,
    xb,
    counts,
    all_counts,
    table_v,
    table_s,
    meta_v,
    meta_s,
    weight_v,
    weight_s,
    w_sem,
    o_sem,
    t_sem,
    cs_sem,
    cr_sem,
    ps_sem,
    pr_sem,
    bs_sem,
    br_sem,
):
    me = lax.axis_index("ep")
    rows, width = tokens.shape
    chunks = width // 128

    names = dict(
        routes=(routes_h, routes),
        tokens=(tokens_h, tokens),
        g_pre=(g_pre_h, g_pre),
        rate=(rate_h, rate_b),
        input=(input_h, input_b),
        wb=(wb_h, wb),
        conv=(conv_h, conv_in),
        taps=(taps_h, taps),
        wg=(wg_h, wg),
        decay=(decay_h, decay),
        recur=(recur_h, recur),
        wm=(wm_h, wm),
        g_post=(g_post_h, g_post),
        g_ffn=(g_ffn_h, g_ffn),
        affinity=(affinity_h, affinity),
        g_out=(g_out_h, g_out),
        eg=(eg_h, eg),
        eu=(eu_h, eu),
        ed=(ed_h, ed),
    )
    loads = {
        k: pltpu.make_async_copy(src, dst, w_sem.at[i])
        for i, (k, (src, dst)) in enumerate(names.items())
    }
    for load in loads.values():
        load.start()

    def ready(*keys):
        for k in keys:
            loads[k].wait()

    scope("greet")
    barrier = pltpu.get_barrier_semaphore()

    def greet(i, carry):
        for j in range(4):
            peer = (me + 4 * i + j) & (n - 1)
            pl.semaphore_signal(barrier, inc=1, device_id=(peer,), device_id_type=MESH)
        return carry

    lax.fori_loop(1, n // 4, greet, 0)
    for j in range(1, 4):
        peer = (me + j) & (n - 1)
        pl.semaphore_signal(barrier, inc=1, device_id=(peer,), device_id_type=MESH)

    scope("tables")
    ready("routes")
    r0, r1 = routes[0:1, :], routes[1:2, :]
    sub = lax.broadcasted_iota(I32, (rows, rows), 0)
    lane = lax.broadcasted_iota(I32, (rows, rows), 1)
    diag = sub == lane

    def column(row):
        return jnp.sum(jnp.where(diag, row, jnp.zeros_like(row)), axis=1, keepdims=True)

    def as_row(col):
        return jnp.sum(jnp.where(diag, col, jnp.zeros_like(col)), axis=0, keepdims=True)

    experts = lax.broadcasted_iota(I32, (rows, n), 1)
    token_of = lax.broadcasted_iota(I32, (rows, n), 0)
    m0, m1 = column(r0) == experts, column(r1) == experts
    both = m0 | m1
    before = dot((lane < sub).astype(F32), both.astype(F32)).astype(I32)
    counts[...] = jnp.sum(both.astype(I32), axis=0, keepdims=True)
    table_v[...] = jnp.zeros_like(table_v)
    for s in range(SLOTS):
        table_v[s : s + 1, :] = jnp.sum(
            jnp.where(both & (before == s), token_of, 0), axis=0, keepdims=True
        )
    for j, m in enumerate((m0, m1)):
        where_at = jnp.sum(jnp.where(m, experts * SLOTS + before, 0), axis=1, keepdims=True)
        table_v[SLOTS + j : SLOTS + j + 1, 0:rows] = as_row(where_at)
    table_copy = pltpu.make_async_copy(table_v, table_s, t_sem)
    table_copy.start()

    scope("blocks")
    ready("rate", "input")
    spread = (
        lax.broadcasted_iota(I32, (64, 256), 1) % 64 == lax.broadcasted_iota(I32, (64, 256), 0)
    ).astype(BF16)
    keep = (lax.broadcasted_iota(I32, (256, 256), 0) // 64) == (
        lax.broadcasted_iota(I32, (256, 256), 1) // 64
    )
    for k, blocks in enumerate((rate_b, input_b)):
        for g in range(4):
            wide = dot(blocks[256 * g : 256 * (g + 1), :], spread)
            bd[k, g] = jnp.where(keep, wide, 0.0).astype(BF16)

    scope("norm")
    ready("tokens", "g_pre")
    tok = tokens[...].astype(F32)
    normed = (tok * inv_rms(tok) * g_pre[...]).astype(BF16)
    scope("branch")
    ready("wb")
    branch = dot(normed, wb[...]).astype(BF16)
    branch_v[...] = branch
    ready("conv", "taps")
    conv_copies = [
        pltpu.make_async_copy(src, conv_out.at[i], o_sem.at[i])
        for i, src in enumerate((conv_in.at[1], conv_in.at[2], branch_v))
    ]
    for copy in conv_copies:
        copy.start()
    conv = branch.astype(F32) * taps[3:4, :]
    for k in range(3):
        conv = conv + conv_in[k].astype(F32) * taps[k : k + 1, :]
    conv_b = conv.astype(BF16)
    scope("gate")
    ready("wg", "decay", "recur")
    gate = dot(normed, wg[...]).astype(BF16).astype(F32)
    d = decay[...]
    soft = jnp.maximum(-d, 0.0) + jnp.log1p(jnp.exp(-jnp.abs(d)))
    merged = []
    for g in range(4):
        cols = slice(256 * g, 256 * (g + 1))
        rate = jax.nn.sigmoid(dot(conv_b[:, cols], bd[0, g]))
        inflow = jax.nn.sigmoid(dot(conv_b[:, cols], bd[1, g]))
        log_decay = -DECAY * rate * soft[:, cols]
        state = jnp.exp(log_decay) * recur[:, cols] + jnp.sqrt(minus_expm1(2.0 * log_decay)) * (
            inflow * conv[:, cols]
        )
        state_v[:, cols] = state
        x = gate[:, cols]
        gelu = 0.5 * x * (1.0 + jnp.tanh(0.7978845608028654 * (x + 0.044715 * (x * x * x))))
        merged.append((state * gelu).astype(BF16))
    merged = jnp.concatenate(merged, axis=1)
    scope("mix")
    ready("wm", "g_post", "g_ffn")
    mix = dot(merged, wm[...]).astype(BF16).astype(F32)
    res = tok + mix * inv_rms(mix) * g_post[...]
    residual[...] = res
    ffn = res * inv_rms(res) * g_ffn[...]

    scope("tiles")
    for c in range(chunks):
        tiles32[pl.ds(c, rows, stride=chunks), :] = ffn[:, 128 * c : 128 * (c + 1)]

    def to_tiles(t, carry):
        at = pl.multiple_of(t * chunks, chunks)
        tiles[t] = tiles32[pl.ds(at, chunks), :].astype(BF16)
        return carry

    lax.fori_loop(0, rows, to_tiles, 0, unroll=8)
    table_copy.wait()

    scope("barrier")
    pl.semaphore_wait(barrier, n - 1)
    scope("send")

    def own_tile(index):
        return tiles[jnp.clip(index, 0, rows - 1)]

    def turned(i):
        return (i * TURN) & (HALF - 1)

    def post(source, target, ssem, rsem, peer):
        pltpu.make_async_remote_copy(
            src_ref=source,
            dst_ref=target,
            send_sem=ssem,
            recv_sem=rsem,
            device_id=(peer,),
            device_id_type=MESH,
        ).start()

    def send_count(peer):
        post(counts, all_counts.at[pl.ds(me, 1)], cs_sem, cr_sem, peer)

    def piped(first, prepare, launch):
        def group(g, start, run):
            for j in range(start, GROUP):
                run(g * GROUP + j)

        def body(g, carry):
            group(g, 0, prepare)
            group(g - 1, 0, launch)
            return carry

        group(0, first, prepare)
        group(1, 0, prepare)
        group(0, first, launch)
        lax.fori_loop(2, HALF // GROUP, body, 0)
        group(HALF // GROUP - 1, 0, launch)

    def pick_rows(half, i):
        peer = moved(me, step_of(half, turned(i)), 1)
        for s in range(SLOTS):
            send[peer, s] = own_tile(table_s[s, peer])
        if half == 0:
            send_count(peer)
            if not (isinstance(i, int) and i == 0):
                send_count(moved(me, step_of(1, turned(i)), 1))

    def send_rows(half, i):
        q = turned(i)
        peer = moved(me, step_of(half, q), 1)
        target = (recv_a, recv_b)[half]
        post(send.at[peer], target.at[q], ps_sem.at[half], pr_sem.at[half], peer)

    for half in range(2):
        piped(half, functools.partial(pick_rows, half), functools.partial(send_rows, half))
    for s in range(SLOTS):
        recv_b[0, s] = own_tile(table_s[s, me])
    all_counts[pl.ds(me, 1), :] = counts[...]
    state_copy = pltpu.make_async_copy(state_v, state_out, o_sem.at[3])
    state_copy.start()

    def total(buffer, blocks, ssem, rsem):
        part = buffer.at[pl.ds(0, blocks)]
        return pltpu.make_async_remote_copy(
            src_ref=part,
            dst_ref=part,
            send_sem=ssem,
            recv_sem=rsem,
            device_id=(me ^ 1,),
            device_id_type=MESH,
        )

    scope("meta")
    count_sum = total(all_counts, n - 1, cs_sem, cr_sem)
    count_sum.wait_recv()
    every = all_counts[...]
    sub_n = lax.broadcasted_iota(I32, (n, n), 0)
    lane_n = lax.broadcasted_iota(I32, (n, n), 1)
    own_col = jnp.sum(jnp.where(lane_n == me, every, 0), axis=1, keepdims=True)
    own_row = jnp.sum(jnp.where(lane_n == sub_n, own_col, 0), axis=0, keepdims=True)
    first_col = jnp.sum(jnp.where(lane_n < sub_n, own_row, 0), axis=1, keepdims=True)
    first_row = jnp.sum(jnp.where(sub_n < lane_n, own_col, 0), axis=0, keepdims=True)
    hit = (first_col <= lane_n) & (lane_n < first_col + own_col)
    step_z = ((me >> 5) - (sub_n >> 5)) & 3
    entry = (
        (step_z >> 1) << 5
        | (((me >> 3) - (sub_n >> 3)) & 3) << 3
        | (((me >> 1) - (sub_n >> 1)) & 3) << 1
        | ((me ^ sub_n) & 1)
    )
    place = SLOTS * entry + lane_n - first_col
    meta_v[...] = jnp.zeros_like(meta_v)
    for half in range(2):
        meta_v[half : half + 1, :] = jnp.sum(
            jnp.where(hit & ((step_z & 1) == 1 - half), place, 0), axis=0, keepdims=True
        )
    for s in range(SLOTS):
        meta_v[2 + s : 3 + s, :] = jnp.minimum(first_row + s, LIMIT - 1)
    meta_copy = pltpu.make_async_copy(meta_v, meta_s, t_sem)
    meta_copy.start()

    base = jnp.sum(jnp.where(sub_n < me, every, 0), axis=0, keepdims=True)
    fits = (base + before) < LIMIT
    ready("affinity")
    a0, a1 = affinity[0:1, :], affinity[1:2, :]
    weight_v[...] = jnp.zeros_like(weight_v)
    for j, (m, a) in enumerate(((m0, a0), (m1, a1))):
        kept = jnp.sum(jnp.where(m & fits, 1.0, 0.0), axis=1, keepdims=True)
        weight_v[j : j + 1, 0:rows] = as_row(kept) * (a / (a0 + a1))
    meta_copy.wait()
    weight_copy = pltpu.make_async_copy(weight_v, weight_s, t_sem)
    weight_copy.start()
    ready("eg", "eu", "ed", "g_out")

    sums = []
    for half, (got, ret) in enumerate(((recv_a, ret_a), (recv_b, ret_b))):
        scope(f"wait{half}")
        rows_sum = total(got, HALF - half, ps_sem.at[half], pr_sem.at[half])
        rows_sum.wait_recv()
        sums.append(rows_sum)
        scope(f"expert{half}")
        got_rows = got.reshape(HALF * SLOTS, chunks, 128)

        def accept(r, carry):
            at = pl.multiple_of(r * chunks, chunks)
            index = jnp.clip(meta_s[half, r], 0, HALF * SLOTS - 1)
            tiles32[pl.ds(at, chunks), :] = got_rows[index].astype(F32)
            return carry

        lax.fori_loop(0, LIMIT, accept, 0, unroll=8)
        for c in range(chunks):
            part = tiles32[pl.ds(c, LIMIT, stride=chunks), :]
            xb[:, 128 * c : 128 * (c + 1)] = part.astype(BF16)
        x = xb[...]
        hidden = (jax.nn.silu(dot(x, eg[...])) * dot(x, eu[...])).astype(BF16)
        result = dot(hidden, ed[...])
        for c in range(chunks):
            tiles32[pl.ds(c, LIMIT, stride=chunks), :] = result[:, 128 * c : 128 * (c + 1)]
        lax.fori_loop(0, LIMIT, to_tiles, 0, unroll=8)
        scope(f"give{half}")

        def result_tile(s, peer):
            return tiles[jnp.clip(meta_s[2 + s, peer], 0, LIMIT - 1)]

        def give(i):
            q = turned(i)
            peer = moved(me, step_of(half, q), -1)
            for s in range(SLOTS):
                ret[q, s] = result_tile(s, peer)

        def send_back(i):
            q = turned(i)
            peer = moved(me, step_of(half, q), -1)
            post(ret.at[q], back.at[me], bs_sem, br_sem, peer)

        piped(half, give, send_back)
    for s in range(SLOTS):
        back[me, s] = result_tile(s, me)
    weight_copy.wait()
    scope("wait2")
    back_sum = total(back, n - 1, bs_sem, br_sem)
    back_sum.wait_recv()

    scope("combine")
    back_rows = back.reshape(n * SLOTS, chunks, 128)

    def combine(t, carry):
        first, second = (
            back_rows[jnp.clip(table_s[SLOTS + j, t], 0, n * SLOTS - 1)].astype(F32)
            * weight_s[j, t]
            for j in range(2)
        )
        at = pl.multiple_of(t * chunks, chunks)
        tiles32[pl.ds(at, chunks), :] = first + second
        return carry

    lax.fori_loop(0, rows, combine, 0, unroll=8)
    parts = [tiles32[pl.ds(c, rows, stride=chunks), :] for c in range(chunks)]
    combined = jnp.concatenate(parts, axis=1)
    out[...] = (residual[...] + combined * inv_rms(combined) * g_out[...]).astype(BF16)
    scope("drain")
    for done in sums:
        done.wait_send()
    back_sum.wait_send()
    count_sum.wait_send()
    for copy in (*conv_copies, state_copy):
        copy.wait()
    scope(None)


def deliver_kernel(a, b, c, a_out, b_out, c_out, a_v, b_v, c_v, sem):
    trips = ((a, a_v, a_out), (b, b_v, b_out), (c, c_v, c_out))
    into = [pltpu.make_async_copy(x, v, sem.at[i]) for i, (x, v, _) in enumerate(trips)]
    onward = [pltpu.make_async_copy(v, y, sem.at[3 + i]) for i, (_, v, y) in enumerate(trips)]
    for copy in into:
        copy.start()
    for first, second in zip(into, onward):
        first.wait()
        second.start()
    for copy in onward:
        copy.wait()


def shards(
    n,
    tokens,
    conv_state,
    recur_state,
    w_branch,
    w_gate,
    conv_taps,
    rate_blocks,
    input_blocks,
    decay_param,
    w_mix,
    gain_pre,
    gain_post,
    gain_ffn,
    gain_out,
    routes,
    affinity,
    w_expert_gate,
    w_expert_up,
    w_expert_down,
):
    rows, width = tokens.shape
    bw = recur_state.shape[1]
    ff = w_expert_gate.shape[2]
    chunks = width // 128
    vmem = pl.BlockSpec(memory_space=pltpu.VMEM)
    hbm = pl.BlockSpec(memory_space=pl.ANY)
    dma = pltpu.SemaphoreType.DMA
    inputs = (
        tokens,
        conv_state.transpose(1, 0, 2),
        recur_state,
        conv_taps,
        decay_param.reshape(1, bw),
        rate_blocks.reshape(bw, -1),
        input_blocks.reshape(bw, -1),
        gain_pre.reshape(1, width),
        gain_post.reshape(1, width),
        gain_ffn.reshape(1, width),
        gain_out.reshape(1, width),
        routes.T,
        affinity.T,
        w_branch,
        w_gate,
        w_mix,
        w_expert_gate.reshape(width, ff),
        w_expert_up.reshape(width, ff),
        w_expert_down.reshape(ff, width),
    )
    results = (
        jax.ShapeDtypeStruct((rows, width), BF16),
        jax.ShapeDtypeStruct((3, rows, bw), BF16),
        jax.ShapeDtypeStruct((rows, bw), F32),
    )
    produced = pl.pallas_call(
        functools.partial(layer_kernel, n),
        out_shape=results,
        in_specs=[hbm] * len(inputs),
        out_specs=(vmem, hbm, hbm),
        scratch_shapes=[pltpu.VMEM(x.shape, x.dtype) for x in inputs]
        + [
            pltpu.VMEM((rows, bw), BF16),
            pltpu.VMEM((rows, bw), F32),
            pltpu.VMEM((2, 4, 256, 256), BF16),
            pltpu.VMEM((rows, width), F32),
            pltpu.VMEM((rows * chunks + chunks, 128), F32),
            pltpu.VMEM((rows, chunks, 128), BF16),
            pltpu.VMEM((n, SLOTS, chunks, 128), BF16),
            pltpu.VMEM((HALF, SLOTS, chunks, 128), BF16),
            pltpu.VMEM((HALF, SLOTS, chunks, 128), BF16),
            pltpu.VMEM((HALF, SLOTS, chunks, 128), BF16),
            pltpu.VMEM((HALF, SLOTS, chunks, 128), BF16),
            pltpu.VMEM((n, SLOTS, chunks, 128), BF16),
            pltpu.VMEM((LIMIT, width), BF16),
            pltpu.VMEM((1, n), I32),
            pltpu.VMEM((n, n), I32),
            pltpu.VMEM((8, 128), I32),
            pltpu.SMEM((8, 128), I32),
            pltpu.VMEM((8, 128), I32),
            pltpu.SMEM((8, 128), I32),
            pltpu.VMEM((8, 128), F32),
            pltpu.SMEM((8, 128), F32),
            dma((len(inputs),)),
            dma((4,)),
            dma,
            dma,
            dma,
            dma((2,)),
            dma((2,)),
            dma,
            dma,
        ],
        compiler_params=pltpu.CompilerParams(
            collective_id=0, has_side_effects=True, vmem_limit_bytes=60 * 1024 * 1024
        ),
        name="layer",
    )(*inputs)
    layer_out, conv_next, state_next = pl.pallas_call(
        deliver_kernel,
        out_shape=results,
        in_specs=[hbm] * 3,
        out_specs=(hbm, hbm, hbm),
        scratch_shapes=[pltpu.VMEM(x.shape, x.dtype) for x in results] + [dma((6,))],
        name="deliver",
    )(*produced)
    return (layer_out, conv_next.transpose(1, 0, 2), state_next)


def solution(mesh):
    row, cube, whole = P("ep", None), P("ep", None, None), P()
    return jax.shard_map(
        functools.partial(shards, mesh.shape["ep"]),
        mesh=mesh,
        in_specs=(row, cube, row) + (whole,) * 11 + (row, row, cube, cube, cube),
        out_specs=(row, cube, row),
        check_vma=False,
    )
```

time: 66.1 us -> 56 us (0.85)
  local copies, waits for them, and re-layouts: 5.11 us -> 0 us
  Pallas kernels: 60.1 us -> 55.2 us
    unnamed x3 -> x0, local copies, waits for them, and re-layouts: 5.11 us -> none
    pallas_call x1 -> x2, Pallas kernels: 60.1 us -> 55.2 us  [the longest x1 53.2 us: shards(): pl.pallas_call(functools.partial(layer_kernel, n), out_shape=results, in_...]
where the time goes in v2:
time: 56 us; the launch traced here: 55.8 us
  Pallas kernels  55.2 us (99%)
  between operations  0.65 us (1%)
    pallas_call x1, Pallas kernels, shards(): pl.pallas_call(functools.partial(layer_kernel, n), out_shape=results, in_...  53.2 us
    pallas_call x1, Pallas kernels, shards(): pl.pallas_call(deliver_kernel, out_shape=results, in_specs=[hbm] * 3, out...  1.96 us

profile of v2, /device:TPU:1, one launch (start us, length us, event | category | flops | bytes accessed | tf_op | source)
XLA Modules:
  0.0 55.8 jit_solution(7817258762355420596)
XLA Ops:
  0.6 53.2 %layer.1 = (bf16[64,2048]{1,0:T(8,128)(2,1)}, bf16[3,64,1024]{2,1,0:T(8,128)(2,1)}, f32[64,1024]{1,0:T(8,128)}) custom-call(bf16[64,2048]{1,0:T(8,128)(2,1)} %tokens_h.1, bf16[3,64,1024]{2,1,0:T(8,128)(2,1)} %bitcast.17, f32[64,1024]{1,0:T(8,128)} %recur_h.1, f32[4,1024]{1,0:T(4,128)} %taps_h.1, f32[1,1024]{1,0:T(1,128)} %bitcast.24, ...), custom_call_target="tpu_custom_call" | custom-call | tf_op jit(solution)/shard_map/layer/pallas_call | solution.py:546
  53.9 2.0 %deliver.1 = (bf16[64,2048]{1,0:T(8,128)(2,1)}, bf16[3,64,1024]{2,1,0:T(8,128)(2,1)}, f32[64,1024]{1,0:T(8,128)}) custom-call(bf16[64,2048]{1,0:T(8,128)(2,1)} %get-tuple-element.9.a, bf16[3,64,1024]{2,1,0:T(8,128)(2,1)} %get-tuple-element.10.b, f32[64,1024]{1,0:T(8,128)} %get-tuple-element.11.c), custom_call_target="tpu_custom_call" | custom-call | tf_op jit(solution)/shard_map/deliver/pallas_call | solution.py:589

commit v3 on v2

--- a/solution.py
+++ b/solution.py
@@ -57,7 +57,7 @@
 
 HALF = 64
 GROUP = 8
-TURN = 37
+TURN = 47
 
 
 def layer_kernel(
@@ -103,8 +103,6 @@
     eg,
     eu,
     ed,
-    branch_v,
-    state_v,
     bd,
     residual,
     tiles32,
@@ -125,7 +123,6 @@
     weight_v,
     weight_s,
     w_sem,
-    o_sem,
     t_sem,
     cs_sem,
     cr_sem,
@@ -138,37 +135,41 @@
     rows, width = tokens.shape
     chunks = width // 128
 
-    names = dict(
-        routes=(routes_h, routes),
-        tokens=(tokens_h, tokens),
-        g_pre=(g_pre_h, g_pre),
-        rate=(rate_h, rate_b),
-        input=(input_h, input_b),
-        wb=(wb_h, wb),
-        conv=(conv_h, conv_in),
-        taps=(taps_h, taps),
-        wg=(wg_h, wg),
-        decay=(decay_h, decay),
-        recur=(recur_h, recur),
-        wm=(wm_h, wm),
-        g_post=(g_post_h, g_post),
-        g_ffn=(g_ffn_h, g_ffn),
-        affinity=(affinity_h, affinity),
-        g_out=(g_out_h, g_out),
-        eg=(eg_h, eg),
-        eu=(eu_h, eu),
-        ed=(ed_h, ed),
-    )
-    loads = {
-        k: pltpu.make_async_copy(src, dst, w_sem.at[i])
-        for i, (k, (src, dst)) in enumerate(names.items())
-    }
-    for load in loads.values():
-        load.start()
+    loads = {}
+
+    def load(key, src, dst):
+        loads[key] = pltpu.make_async_copy(src, dst, w_sem.at[len(loads)])
+        loads[key].start()
 
     def ready(*keys):
         for k in keys:
             loads[k].wait()
+
+    def load_columns(g):
+        cols = pl.ds(256 * g, 256)
+        load(f"wb{g}", wb_h.at[:, cols], wb.at[:, cols])
+        load(f"wg{g}", wg_h.at[:, cols], wg.at[:, cols])
+
+    load("tokens", tokens_h, tokens)
+    load("g_pre", g_pre_h, g_pre)
+    load("routes", routes_h, routes)
+    load("rate", rate_h, rate_b)
+    load("input", input_h, input_b)
+    load_columns(0)
+    load("conv", conv_h, conv_in)
+    load("taps", taps_h, taps)
+    load("decay", decay_h, decay)
+    load("recur", recur_h, recur)
+    load_columns(1)
+    load_columns(2)
+    load_columns(3)
+    for h in range(2):
+        part = pl.ds(512 * h, 512)
+        load(f"wm{h}", wm_h.at[part], wm.at[part])
+    load("g_post", g_post_h, g_post)
+    load("g_ffn", g_ffn_h, g_ffn)
+    load("affinity", affinity_h, affinity)
+    load("g_out", g_out_h, g_out)
 
     scope("greet")
     barrier = pltpu.get_barrier_semaphore()
@@ -184,8 +185,23 @@
         peer = (me + j) & (n - 1)
         pl.semaphore_signal(barrier, inc=1, device_id=(peer,), device_id_type=MESH)
 
-    scope("tables")
-    ready("routes")
+    scope("norm")
+    ready("tokens", "g_pre", "routes", "rate", "input")
+    tok = tokens[...].astype(F32)
+    normed = (tok * inv_rms(tok) * g_pre[...]).astype(BF16)
+    scope("first")
+    ready("wb0", "wg0", "conv", "taps", "decay", "recur")
+    spread = (
+        lax.broadcasted_iota(I32, (64, 256), 1) % 64 == lax.broadcasted_iota(I32, (64, 256), 0)
+    ).astype(BF16)
+    keep = (lax.broadcasted_iota(I32, (256, 256), 0) // 64) == (
+        lax.broadcasted_iota(I32, (256, 256), 1) // 64
+    )
+    for k, blocks in enumerate((rate_b, input_b)):
+        for g in range(4):
+            wide = dot(blocks[256 * g : 256 * (g + 1), :], spread)
+            bd[k, g] = jnp.where(keep, wide, 0.0).astype(BF16)
+
     r0, r1 = routes[0:1, :], routes[1:2, :]
     sub = lax.broadcasted_iota(I32, (rows, rows), 0)
     lane = lax.broadcasted_iota(I32, (rows, rows), 1)
@@ -214,60 +230,50 @@
     table_copy = pltpu.make_async_copy(table_v, table_s, t_sem)
     table_copy.start()
 
-    scope("blocks")
-    ready("rate", "input")
-    spread = (
-        lax.broadcasted_iota(I32, (64, 256), 1) % 64 == lax.broadcasted_iota(I32, (64, 256), 0)
-    ).astype(BF16)
-    keep = (lax.broadcasted_iota(I32, (256, 256), 0) // 64) == (
-        lax.broadcasted_iota(I32, (256, 256), 1) // 64
-    )
-    for k, blocks in enumerate((rate_b, input_b)):
-        for g in range(4):
-            wide = dot(blocks[256 * g : 256 * (g + 1), :], spread)
-            bd[k, g] = jnp.where(keep, wide, 0.0).astype(BF16)
-
-    scope("norm")
-    ready("tokens", "g_pre")
-    tok = tokens[...].astype(F32)
-    normed = (tok * inv_rms(tok) * g_pre[...]).astype(BF16)
-    scope("branch")
-    ready("wb")
-    branch = dot(normed, wb[...]).astype(BF16)
-    branch_v[...] = branch
-    ready("conv", "taps")
-    conv_copies = [
-        pltpu.make_async_copy(src, conv_out.at[i], o_sem.at[i])
-        for i, src in enumerate((conv_in.at[1], conv_in.at[2], branch_v))
-    ]
-    for copy in conv_copies:
-        copy.start()
-    conv = branch.astype(F32) * taps[3:4, :]
-    for k in range(3):
-        conv = conv + conv_in[k].astype(F32) * taps[k : k + 1, :]
-    conv_b = conv.astype(BF16)
-    scope("gate")
-    ready("wg", "decay", "recur")
-    gate = dot(normed, wg[...]).astype(BF16).astype(F32)
-    d = decay[...]
-    soft = jnp.maximum(-d, 0.0) + jnp.log1p(jnp.exp(-jnp.abs(d)))
+    def project(g):
+        cols = slice(256 * g, 256 * (g + 1))
+        return dot(normed, wb[:, cols]).astype(BF16), dot(normed, wg[:, cols]).astype(BF16)
+
+    def advance(g, branch, gate):
+        cols = slice(256 * g, 256 * (g + 1))
+        conv_out[0, :, cols] = conv_in[1, :, cols]
+        conv_out[1, :, cols] = conv_in[2, :, cols]
+        conv_out[2, :, cols] = branch
+        conv = branch.astype(F32) * taps[3:4, cols]
+        for k in range(3):
+            conv = conv + conv_in[k, :, cols].astype(F32) * taps[k : k + 1, cols]
+        conv_b = conv.astype(BF16)
+        d = decay[:, cols]
+        soft = jnp.maximum(-d, 0.0) + jnp.log1p(jnp.exp(-jnp.abs(d)))
+        rate = jax.nn.sigmoid(dot(conv_b, bd[0, g]))
+        inflow = jax.nn.sigmoid(dot(conv_b, bd[1, g]))
+        log_decay = -DECAY * rate * soft
+        state = jnp.exp(log_decay) * recur[:, cols] + jnp.sqrt(minus_expm1(2.0 * log_decay)) * (
+            inflow * conv
+        )
+        state_out[:, cols] = state
+        x = gate.astype(F32)
+        gelu = 0.5 * x * (1.0 + jnp.tanh(0.7978845608028654 * (x + 0.044715 * (x * x * x))))
+        return (state * gelu).astype(BF16)
+
     merged = []
-    for g in range(4):
-        cols = slice(256 * g, 256 * (g + 1))
-        rate = jax.nn.sigmoid(dot(conv_b[:, cols], bd[0, g]))
-        inflow = jax.nn.sigmoid(dot(conv_b[:, cols], bd[1, g]))
-        log_decay = -DECAY * rate * soft[:, cols]
-        state = jnp.exp(log_decay) * recur[:, cols] + jnp.sqrt(minus_expm1(2.0 * log_decay)) * (
-            inflow * conv[:, cols]
-        )
-        state_v[:, cols] = state
-        x = gate[:, cols]
-        gelu = 0.5 * x * (1.0 + jnp.tanh(0.7978845608028654 * (x + 0.044715 * (x * x * x))))
-        merged.append((state * gelu).astype(BF16))
-    merged = jnp.concatenate(merged, axis=1)
+    projected = project(0)
+    scope("project")
+    for g in range(1, 4):
+        ready(f"wb{g}", f"wg{g}")
+        following = project(g)
+        merged.append(advance(g - 1, *projected))
+        projected = following
     scope("mix")
-    ready("wm", "g_post", "g_ffn")
-    mix = dot(merged, wm[...]).astype(BF16).astype(F32)
+    ready("wm0")
+    half_mix = dot(jnp.concatenate(merged[:2], axis=1), wm[:512, :])
+    merged.append(advance(3, *projected))
+    ready("wm1", "g_post", "g_ffn")
+    mix = half_mix + dot(jnp.concatenate(merged[2:], axis=1), wm[512:, :])
+    mix = mix.astype(BF16).astype(F32)
+    load("eg", eg_h, eg)
+    load("eu", eu_h, eu)
+    load("ed", ed_h, ed)
     res = tok + mix * inv_rms(mix) * g_post[...]
     residual[...] = res
     ffn = res * inv_rms(res) * g_ffn[...]
@@ -343,8 +349,6 @@
     for s in range(SLOTS):
         recv_b[0, s] = own_tile(table_s[s, me])
     all_counts[pl.ds(me, 1), :] = counts[...]
-    state_copy = pltpu.make_async_copy(state_v, state_out, o_sem.at[3])
-    state_copy.start()
 
     def total(buffer, blocks, ssem, rsem):
         part = buffer.at[pl.ds(0, blocks)]
@@ -470,21 +474,15 @@
         done.wait_send()
     back_sum.wait_send()
     count_sum.wait_send()
-    for copy in (*conv_copies, state_copy):
-        copy.wait()
     scope(None)
 
 
-def deliver_kernel(a, b, c, a_out, b_out, c_out, a_v, b_v, c_v, sem):
-    trips = ((a, a_v, a_out), (b, b_v, b_out), (c, c_v, c_out))
-    into = [pltpu.make_async_copy(x, v, sem.at[i]) for i, (x, v, _) in enumerate(trips)]
-    onward = [pltpu.make_async_copy(v, y, sem.at[3 + i]) for i, (_, v, y) in enumerate(trips)]
-    for copy in into:
+def deliver_kernel(a, b, c, a_out, b_out, c_out, sem):
+    trips = ((a, a_out), (b, b_out), (c, c_out))
+    copies = [pltpu.make_async_copy(x, y, sem.at[i]) for i, (x, y) in enumerate(trips)]
+    for copy in copies:
         copy.start()
-    for first, second in zip(into, onward):
-        first.wait()
-        second.start()
-    for copy in onward:
+    for copy in copies:
         copy.wait()
 
 
@@ -545,13 +543,11 @@
     )
     produced = pl.pallas_call(
         functools.partial(layer_kernel, n),
-        out_shape=results,
+        out_shape=tuple(pltpu.VMEM(x.shape, x.dtype) for x in results),
         in_specs=[hbm] * len(inputs),
-        out_specs=(vmem, hbm, hbm),
+        out_specs=(vmem, vmem, vmem),
         scratch_shapes=[pltpu.VMEM(x.shape, x.dtype) for x in inputs]
         + [
-            pltpu.VMEM((rows, bw), BF16),
-            pltpu.VMEM((rows, bw), F32),
             pltpu.VMEM((2, 4, 256, 256), BF16),
             pltpu.VMEM((rows, width), F32),
             pltpu.VMEM((rows * chunks + chunks, 128), F32),
@@ -571,8 +567,7 @@
             pltpu.SMEM((8, 128), I32),
             pltpu.VMEM((8, 128), F32),
             pltpu.SMEM((8, 128), F32),
-            dma((len(inputs),)),
-            dma((4,)),
+            dma((26,)),
             dma,
             dma,
             dma,
@@ -589,11 +584,11 @@
     layer_out, conv_next, state_next = pl.pallas_call(
         deliver_kernel,
         out_shape=results,
-        in_specs=[hbm] * 3,
+        in_specs=[vmem] * 3,
         out_specs=(hbm, hbm, hbm),
-        scratch_shapes=[pltpu.VMEM(x.shape, x.dtype) for x in results] + [dma((6,))],
+        scratch_shapes=[dma((3,))],
         name="deliver",
-    )(*produced)
+    )(*(pltpu.with_memory_space_constraint(x, pltpu.VMEM) for x in produced))
     return (layer_out, conv_next.transpose(1, 0, 2), state_next)
 
 

time: 56 us -> 53.2 us (0.950)
  Pallas kernels: 55.2 us -> 52.5 us
    pallas_call x2, Pallas kernels: 55.2 us -> 52.5 us  [the longest x1 51.5 us: shards(): pl.pallas_call(functools.partial(layer_kernel, n), out_shape=tuple((pltpu...]
where the time goes in v3:
time: 53.2 us; the launch traced here: 53.1 us
  Pallas kernels  52.5 us (99%)
  between operations  0.65 us (1%)
    pallas_call x1, Pallas kernels, shards(): pl.pallas_call(functools.partial(layer_kernel, n), out_shape=tuple((pltpu...  51.5 us

profile of v3, /device:TPU:1, one launch (start us, length us, event | category | flops | bytes accessed | tf_op | source)
XLA Modules:
  0.0 53.1 jit_solution(14873345093738459979)
XLA Ops:
  0.6 51.5 %layer.1 = (bf16[64,2048]{1,0:T(8,128)(2,1)S(1)}, bf16[3,64,1024]{2,1,0:T(8,128)(2,1)S(1)}, f32[64,1024]{1,0:T(8,128)S(1)}) custom-call(bf16[64,2048]{1,0:T(8,128)(2,1)} %tokens_h.1, bf16[3,64,1024]{2,1,0:T(8,128)(2,1)} %bitcast.17, f32[64,1024]{1,0:T(8,128)} %recur_h.1, f32[4,1024]{1,0:T(4,128)} %taps_h.1, f32[1,1024]{1,0:T(1,128)} %bitcast.24, ...), custom_call_target="tpu_custom_call" | custom-call | tf_op jit(solution)/shard_map/layer/pallas_call | solution.py:544
  52.2 0.9 %deliver.1 = (bf16[64,2048]{1,0:T(8,128)(2,1)}, bf16[3,64,1024]{2,1,0:T(8,128)(2,1)}, f32[64,1024]{1,0:T(8,128)}) custom-call(bf16[64,2048]{1,0:T(8,128)(2,1)S(1)} %get-tuple-element.9.a, bf16[3,64,1024]{2,1,0:T(8,128)(2,1)S(1)} %get-tuple-element.10.b, f32[64,1024]{1,0:T(8,128)S(1)} %get-tuple-element.11.c), custom_call_target="tpu_custom_call" | custom-call | tf_op jit(solution)/shard_map/deliver/pallas_call | solution.py:584

commit v4 on v3

--- a/solution.py
+++ b/solution.py
@@ -58,6 +58,7 @@
 HALF = 64
 GROUP = 8
 TURN = 47
+TURN_BACK = 15
 
 
 def layer_kernel(
@@ -433,14 +434,22 @@
         def result_tile(s, peer):
             return tiles[jnp.clip(meta_s[2 + s, peer], 0, LIMIT - 1)]
 
+        step_1 = moved(me, (0, 0, 0, 1), 1)
+        q_1 = (step_1 >> 6) << 5 | (step_1 & 31)
+        lead = (q_1 * TURN_BACK) & (HALF - 1)
+        lead = jnp.where(lead < half, half, lead)
+
+        def turned_back(i):
+            return turned(jnp.where(i == half, lead, jnp.where(i == lead, half, i)))
+
         def give(i):
-            q = turned(i)
+            q = turned_back(i)
             peer = moved(me, step_of(half, q), -1)
             for s in range(SLOTS):
                 ret[q, s] = result_tile(s, peer)
 
         def send_back(i):
-            q = turned(i)
+            q = turned_back(i)
             peer = moved(me, step_of(half, q), -1)
             post(ret.at[q], back.at[me], bs_sem, br_sem, peer)
 

time: 53.2 us -> 52 us (0.977)
  Pallas kernels: 52.5 us -> 51.2 us
    pallas_call x1, Pallas kernels: 51.5 us -> 50.3 us  [shards(): pl.pallas_call(functools.partial(layer_kernel, n), out_shape=tuple((pltpu...]
where the time goes in v4:
time: 52 us; the launch traced here: 51.9 us
  Pallas kernels  51.2 us (98%)
  between operations  0.65 us (1%)
    pallas_call x1, Pallas kernels, shards(): pl.pallas_call(functools.partial(layer_kernel, n), out_shape=tuple((pltpu...  50.3 us

profile of v4, /device:TPU:1, one launch (start us, length us, event | category | flops | bytes accessed | tf_op | source)
XLA Modules:
  0.0 51.9 jit_solution(14810887241445616522)
XLA Ops:
  0.6 50.3 %layer.1 = (bf16[64,2048]{1,0:T(8,128)(2,1)S(1)}, bf16[3,64,1024]{2,1,0:T(8,128)(2,1)S(1)}, f32[64,1024]{1,0:T(8,128)S(1)}) custom-call(bf16[64,2048]{1,0:T(8,128)(2,1)} %tokens_h.1, bf16[3,64,1024]{2,1,0:T(8,128)(2,1)} %bitcast.17, f32[64,1024]{1,0:T(8,128)} %recur_h.1, f32[4,1024]{1,0:T(4,128)} %taps_h.1, f32[1,1024]{1,0:T(1,128)} %bitcast.24, ...), custom_call_target="tpu_custom_call" | custom-call | tf_op jit(solution)/shard_map/layer/pallas_call | solution.py:553
  50.9 0.9 %deliver.1 = (bf16[64,2048]{1,0:T(8,128)(2,1)}, bf16[3,64,1024]{2,1,0:T(8,128)(2,1)}, f32[64,1024]{1,0:T(8,128)}) custom-call(bf16[64,2048]{1,0:T(8,128)(2,1)S(1)} %get-tuple-element.9.a, bf16[3,64,1024]{2,1,0:T(8,128)(2,1)S(1)} %get-tuple-element.10.b, f32[64,1024]{1,0:T(8,128)S(1)} %get-tuple-element.11.c), custom_call_target="tpu_custom_call" | custom-call | tf_op jit(solution)/shard_map/deliver/pallas_call | solution.py:593

commit v5 on v4

--- a/solution.py
+++ b/solution.py
@@ -56,7 +56,7 @@
 
 
 HALF = 64
-GROUP = 8
+GROUP = 4
 TURN = 47
 TURN_BACK = 15
 

time: 52 us -> 52 us (level)
  no operation moved by 1% of the time
where the time goes in v5:
time: 52 us; the launch traced here: 51.5 us
  Pallas kernels  50.8 us (98%)
  between operations  0.65 us (1%)
    pallas_call x1, Pallas kernels, shards(): pl.pallas_call(functools.partial(layer_kernel, n), out_shape=tuple((pltpu...  49.9 us

profile of v5, /device:TPU:1, one launch (start us, length us, event | category | flops | bytes accessed | tf_op | source)
XLA Modules:
  0.0 51.5 jit_solution(10470219369450976402)
XLA Ops:
  0.6 49.9 %layer.1 = (bf16[64,2048]{1,0:T(8,128)(2,1)S(1)}, bf16[3,64,1024]{2,1,0:T(8,128)(2,1)S(1)}, f32[64,1024]{1,0:T(8,128)S(1)}) custom-call(bf16[64,2048]{1,0:T(8,128)(2,1)} %tokens_h.1, bf16[3,64,1024]{2,1,0:T(8,128)(2,1)} %bitcast.17, f32[64,1024]{1,0:T(8,128)} %recur_h.1, f32[4,1024]{1,0:T(4,128)} %taps_h.1, f32[1,1024]{1,0:T(1,128)} %bitcast.24, ...), custom_call_target="tpu_custom_call" | custom-call | tf_op jit(solution)/shard_map/layer/pallas_call | solution.py:553
  50.5 0.9 %deliver.1 = (bf16[64,2048]{1,0:T(8,128)(2,1)}, bf16[3,64,1024]{2,1,0:T(8,128)(2,1)}, f32[64,1024]{1,0:T(8,128)}) custom-call(bf16[64,2048]{1,0:T(8,128)(2,1)S(1)} %get-tuple-element.9.a, bf16[3,64,1024]{2,1,0:T(8,128)(2,1)S(1)} %get-tuple-element.10.b, f32[64,1024]{1,0:T(8,128)S(1)} %get-tuple-element.11.c), custom_call_target="tpu_custom_call" | custom-call | tf_op jit(solution)/shard_map/deliver/pallas_call | solution.py:593
